TPU v7x, 32 devices: a whole 2x2x4 slice. The times are simulated.
32 devices in a mesh: sp: 8 (over z, y), dp: 4 (over x, core).
Axes of the slice: x: 2, y: 2, z: 4, core: 2. Of those that a mesh axis runs over, the one named last changes fastest.
Arguments:
- queries: bfloat16 [4, 1024, 2048], P('dp', 'sp'), may hold values from -40 to 40
- keys: bfloat16 [4, 1024, 512], P('dp', 'sp'), may hold values from -8 to 8
- values: bfloat16 [4, 1024, 512], P('dp', 'sp'), may hold values from -6 to 6
- lambdas: float32 [16], replicated, may hold values from 0.3 to 0.8
- value_gain: float32 [128], replicated, may hold values from 0.1 to 1.9
- out_weight: bfloat16 [2048, 4096], P(None, ('sp', 'dp')), may hold values from -0.125 to 0.125
Outputs:
- mixed: bfloat16 [4, 1024, 4096], P('dp', 'sp')
All inputs are finite; a program needn't handle non-finite values.
Results may differ from a plain program's by a relative error of at most 0.0087.
Values may be sent and summed in bfloat16 or wider, within the bound.
A program may use at most 128 MiB of HBM per device.

v0:
```python
import jax
import jax.numpy as jnp
from jax import lax
from jax.sharding import PartitionSpec as P

HEADS = 16
KV_HEADS = 4
HEAD_DIM = 64
VALUE_DIM = 128
rope_base = 500000.0
output_scale = 0.8
norm_eps = 1e-05


def swapped(block, axis, distance):
    count = lax.axis_size(axis)
    route = []
    for low in range(count):
        high = low | 1 << distance
        if high != low and high < count:
            route += [(low, high), (high, low)]
    return lax.ppermute(block, axis, route)


def rotate(parts, positions):
    width = parts.shape[-1]
    half = width // 2
    freqs = rope_base ** (-jnp.arange(0, width, 2, dtype=jnp.float32) / width)
    angles = positions[:, None] * freqs[None, :]
    shape = (angles.shape[0],) + (1,) * (parts.ndim - 2) + (half,)
    cosine = jnp.cos(angles).reshape(shape)
    sine = jnp.sin(angles).reshape(shape)
    first = parts[..., :half]
    second = parts[..., half:]
    return jnp.concatenate([first * cosine - second * sine, second * cosine + first * sine], -1)


def gather_group(key_value, group_size):
    tok_rows = key_value.shape[0]
    sub_rows = tok_rows // group_size
    width = key_value.shape[-1]
    arranged = key_value.reshape(group_size, sub_rows, KV_HEADS, 2, width)
    arranged = jnp.transpose(arranged, (2, 0, 1, 3, 4)).reshape(
        group_size * KV_HEADS, sub_rows, 2, width
    )
    received = lax.all_to_all(arranged, "sp", split_axis=0, concat_axis=1, tiled=True)
    held = received.reshape(1, -1, sub_rows, 2, width)
    device_index = lax.axis_index("sp")
    for bit_number in range(group_size.bit_length() - 1):
        partner = swapped(held, "sp", bit_number)
        upper = device_index // 2**bit_number % 2 == 1
        held = jnp.concatenate(
            [jnp.where(upper, partner, held), jnp.where(upper, held, partner)], 0
        )
    ordered = jnp.transpose(held, (1, 0, 2, 3, 4)).reshape(-1, 2, width)
    return (ordered[:, 0], ordered[:, 1])


def attend(query_rot, key_rot, value_whole, lambda_heads, value_gain):
    seqlen = key_rot.shape[0]
    block_rows = min(512, seqlen)
    count = seqlen // block_rows
    score_scale = query_rot.shape[-1] ** (-0.5)
    outputs = []
    for block_index in range(count):
        start = block_index * block_rows
        reach = start + block_rows
        query_block = query_rot[start:reach]
        key_part = key_rot[:reach]
        value_part = value_whole[:reach]
        scores = (
            jnp.einsum("qhmd,kmd->hmqk", query_block, key_part, preferred_element_type=jnp.float32)
            * score_scale
        )
        allowed = jnp.arange(reach)[None, :] <= (start + jnp.arange(block_rows))[:, None]
        scores = jnp.where(allowed[None, None], scores, -jnp.inf)
        row_top = jnp.max(scores, -1, keepdims=True)
        raised = jnp.exp(scores - row_top)
        maps = raised / jnp.sum(raised, -1, keepdims=True)
        weights = (maps[:, 0] - lambda_heads[:, None, None] * maps[:, 1]).astype(jnp.bfloat16)
        outputs.append(
            jnp.einsum("hqk,ke->qhe", weights, value_part, preferred_element_type=jnp.float32)
        )
    head_values = jnp.concatenate(outputs, 0)
    squares = jnp.mean(head_values * head_values, -1, keepdims=True)
    normed = head_values * lax.rsqrt(squares + norm_eps) * value_gain * output_scale
    return normed.astype(jnp.bfloat16)


def shards(queries, keys, values, lambdas, value_gain, out_weight):
    tok_rows = queries.shape[1]
    sp_count = lax.axis_size("sp")
    group_size = sp_count // KV_HEADS
    per_device = HEADS // sp_count
    query_split = queries[0].reshape(tok_rows, HEADS, 2 * HEAD_DIM)
    key_split = keys[0].reshape(tok_rows, KV_HEADS, 2 * HEAD_DIM)
    value_split = values[0].reshape(tok_rows, KV_HEADS, VALUE_DIM)
    query_heads = lax.all_to_all(query_split, "sp", split_axis=1, concat_axis=0, tiled=True)
    key_whole, value_whole = gather_group(jnp.stack([key_split, value_split], 2), group_size)
    seqlen = query_heads.shape[0]
    positions = jnp.arange(seqlen, dtype=jnp.float32)
    query_rot = rotate(
        query_heads.reshape(seqlen, per_device, 2, HEAD_DIM).astype(jnp.float32), positions
    ).astype(jnp.bfloat16)
    key_rot = rotate(key_whole.reshape(seqlen, 2, HEAD_DIM).astype(jnp.float32), positions).astype(
        jnp.bfloat16
    )
    lambda_heads = lax.dynamic_slice_in_dim(
        lambdas, lax.axis_index("sp") * per_device, per_device, 0
    )
    head_out = attend(query_rot, key_rot, value_whole, lambda_heads, value_gain)
    heads_local = lax.all_to_all(
        head_out.reshape(seqlen, per_device * VALUE_DIM),
        "sp",
        split_axis=0,
        concat_axis=1,
        tiled=True,
    )
    mixed = jnp.dot(
        heads_local,
        lax.all_gather(out_weight, ("sp", "dp"), axis=1, tiled=True),
        preferred_element_type=jnp.float32,
    ).astype(jnp.bfloat16)
    return mixed[None]


def solution(mesh):
    return jax.shard_map(
        shards,
        mesh=mesh,
        in_specs=(
            P("dp", "sp", None),
            P("dp", "sp", None),
            P("dp", "sp", None),
            P(),
            P(),
            P(None, ("sp", "dp")),
        ),
        out_specs=P("dp", "sp", None),
        check_vma=False,
    )
```

profile of v0, /device:TPU:0, one launch (start us, length us, event | category | flops | bytes accessed | tf_op | source)
XLA Modules:
  0.0 182.8 jit_solution(17417908235289656183)
XLA Ops:
  6.5 0.0 copy-start
  6.5 0.0 copy-start.2
  6.5 0.0 all-gather.2.cloned.1.call-start
  6.5 0.7 all-gather.2.cloned.1.call-update
  7.3 0.9 stack.7
  8.2 0.9 stack.8
  9.2 0.7 pad_maximum_fusion.3
  9.9 7.3 %all-to-all-start = ((bf16[8,64,2,128]{3,1,2,0:T(8,128)(2,1)}), bf16[8,64,2,128]{3,1,2,0:T(8,128)(2,1)S(1)}, u32[]{:S(2)}, u32[]{:S(2)}) async-start(bf16[8,64,2,128]{3,1,2,0:T(8,128)(2,1)} %bitcast.1), calls=%async_computation | async-start | bytes 524288 | tf_op jit(solution)/shard_map/all_to_all | solution.py:46
  17.2 2.0 %copy.40 = bf16[1,128,2048]{1,2,0:T(8,128)(2,1)} copy(bf16[1,128,2048]{2,1,0:T(8,128)(2,1)} %param.6) | data formatting | bytes 1048576 | tf_op args[0]
  19.3 0.5 fusion.39
  19.8 0.4 iota_compare_fusion
  20.2 6.0 %all-to-all-done = bf16[8,64,2,128]{3,1,2,0:T(8,128)(2,1)S(1)} async-done(((bf16[8,64,2,128]{3,1,2,0:T(8,128)(2,1)}), bf16[8,64,2,128]{3,1,2,0:T(8,128)(2,1)S(1)}, u32[]{:S(2)}, u32[]{:S(2)}) %all-to-all-start) | async-done | bytes 262176 | tf_op jit(solution)/shard_map/all_to_all | solution.py:46
  26.3 3.5 %all-to-all-start.1 = ((bf16[128,16,128]{0,2,1:T(8,128)(2,1)}), bf16[128,16,128]{0,2,1:T(8,128)(2,1)S(1)}, u32[]{:S(2)}, u32[]{:S(2)}) async-start(bf16[128,16,128]{0,2,1:T(8,128)(2,1)} %bitcast.10), calls=%async_computation.1 | async-start | bytes 1048576 | tf_op jit(solution)/shard_map/all_to_all | solution.py:98
  29.8 2.0 %collective-permute-start = (bf16[1,8,64,2,128]{4,2,3,1,0:T(8,128)(2,1)S(1)}, bf16[1,8,64,2,128]{4,2,3,1,0:T(8,128)(2,1)S(1)}, u32[]{:S(2)}, u32[]{:S(2)}) collective-permute-start(bf16[1,8,64,2,128]{4,2,3,1,0:T(8,128)(2,1)S(1)} %bitcast.118), channel_id=1, source_target_pairs={{0,4},{4,0},{8,12},{12,8},{16,20},{20,16},{24,28},{28,24},{1,5},{5... | collective-permute-start | bytes 786440 | tf_op jit(solution)/shard_map/ppermute | solution.py:22
  31.8 0.0 copy-done
  31.8 0.8 iota_compare_fusion.1
  32.5 0.0 copy-done.2
  32.5 0.1 dynamic_slice.3
  32.6 13.4 %collective-permute-done = bf16[1,8,64,2,128]{4,2,3,1,0:T(8,128)(2,1)S(1)} collective-permute-done((bf16[1,8,64,2,128]{4,2,3,1,0:T(8,128)(2,1)S(1)}, bf16[1,8,64,2,128]{4,2,3,1,0:T(8,128)(2,1)S(1)}, u32[]{:S(2)}, u32[]{:S(2)}) %collective-permute-start) | collective-permute-done | bytes 262176 | tf_op jit(solution)/shard_map/ppermute | solution.py:22
  46.1 0.1 maximum_bitcast_fusion
  46.2 0.2 copy.39
  46.4 0.7 subtract_convert_fusion.1
  47.2 6.0 %all-to-all-done.1 = bf16[128,16,128]{0,2,1:T(8,128)(2,1)S(1)} async-done(((bf16[128,16,128]{0,2,1:T(8,128)(2,1)}), bf16[128,16,128]{0,2,1:T(8,128)(2,1)S(1)}, u32[]{:S(2)}, u32[]{:S(2)}) %all-to-all-start.1) | async-done | bytes 524320 | tf_op jit(solution)/shard_map/all_to_all | solution.py:98
  53.1 0.1 convert_element_type.55
  53.2 0.6 copy.42
  53.9 0.2 reshape.176
  54.0 0.1 fusion.63
  54.1 0.1 subtract_convert_fusion
  54.3 4.5 %fusion.69 = (f32[2,2,512]{2,0,1:T(2,128)S(1)}, f32[2,2,512,512]{2,3,0,1:T(8,128)}) fusion(pred[512,512]{0,1:T(8,128)(4,1)} %iota_compare_fusion.1, bf16[1024,2,32]{0,2,1:T(8,128)(2,1)S(1)} %get-tuple-element.9, bf16[1024,2,32]{0,2,1:T(8,128)(2,1)} %get-tuple-element.10, bf16[1024,2,2,32]{0,3,1,2:T(8,128)(2,1)S(1)} %get-tuple-element.5, ...), kind=kOutput, calls=%fused_computation.77 | convolution fusion | flops 139198976 | bytes 5251072 | tf_op jit(solution)/shard_map/sub | solution.py:78
  58.8 0.0 copy-start.1
  58.8 3.0 %broadcast_divide_fusion.1 = f32[2,2,512,512]{2,3,0,1:T(8,128)S(1)} fusion(f32[2,2,512,512]{2,3,0,1:T(8,128)} %get-tuple-element.18, f32[2,2,512]{2,0,1:T(2,128)S(1)} %get-tuple-element.17), kind=kLoop, calls=%fused_computation.22 | loop fusion | flops 1048576 | bytes 8396800 | tf_op jit(solution)/shard_map/div | solution.py:79
  61.9 0.4 fusion.19
  62.3 0.0 copy-done.1
  62.3 5.3 %fusion.64 = (f32[2,2,512]{2,0,1:T(2,128)S(1)}, f32[2,2,512,1024]{2,3,0,1:T(8,128)}) fusion(pred[512,1024]{0,1:T(8,128)(4,1)S(1)} %iota_compare_fusion, bf16[1024,2,32]{0,2,1:T(8,128)(2,1)S(1)} %copy-done.1, bf16[1024,2,32]{0,2,1:T(8,128)(2,1)S(1)} %get-tuple-element.9, bf16[1024,2,2,32]{0,3,1,2:T(8,128)(2,1)S(1)} %get-tuple-element.6, ...), kind=kOutput, calls=%fused_computation.76 | convolution fusion | flops 277873664 | bytes 9707520 | tf_op jit(solution)/shard_map/sub | solution.py:78
  67.6 4.5 %broadcast_divide_fusion = f32[2,2,512,1024]{2,3,0,1:T(8,128)S(1)} fusion(f32[2,2,512,1024]{2,3,0,1:T(8,128)} %get-tuple-element.16, f32[2,2,512]{2,0,1:T(2,128)S(1)} %get-tuple-element.15), kind=kLoop, calls=%fused_computation.11 | loop fusion | flops 2097152 | bytes 16785408 | tf_op jit(solution)/shard_map/div | solution.py:79
  72.1 0.6 fusion.15
  72.8 0.1 fusion.21
  72.9 0.1 mul.266
  73.0 0.2 copy.61
  73.2 0.4 copy.50
  73.6 0.2 copy.48
  73.8 0.2 copy.49
  74.0 0.1 pad_maximum_fusion
  74.1 0.2 multiply_convert_fusion
  74.3 32.6 %all_to_all.34 = bf16[8,128,256]{2,1,0:T(8,128)(2,1)S(1)} all-to-all(bf16[8,128,256]{2,1,0:T(8,128)(2,1)S(1)} %multiply_convert_fusion), channel_id=1, replica_groups=mesh['sp'=8,'dp'=4] {'sp'}, dimensions={0} | all-to-all | bytes 1048576 | tf_op jit(solution)/shard_map/all_to_all | solution.py:112
  106.9 0.3 copy.51
  107.2 59.7 %all-gather.2.cloned.1.call-done = bf16[2048,4096]{1,0:T(8,128)(2,1)} async-done(((bf16[2048,128]{1,0:T(8,128)(2,1)}), bf16[2048,4096]{1,0:T(8,128)(2,1)}) %all-gather.2.cloned.1.call-update) | async-done | bytes 16777232 | tf_op jit(solution)/shard_map/all_gather | solution.py:121
  166.8 9.1 %fusion.3 = bf16[1,128,4096]{2,1,0:T(8,128)(2,1)} fusion(bf16[128,2048]{0,1:T(8,128)(2,1)S(1)} %bitcast.112, bf16[2048,4096]{1,0:T(8,128)(2,1)} %all-gather.2.cloned.1.call-done), kind=kOutput, calls=%fused_computation.6 | convolution fusion | flops 2148007936 | bytes 18350080 | tf_op jit(solution)/shard_map/dot_general | solution.py:119
  (9 shorter events, 0.2 us)
Async XLA Ops:
  6.5 25.2 %copy-start = (f32[128]{0:T(128)S(1)}, f32[128]{0:T(128)}, u32[]{:S(2)}) copy-start(f32[128]{0:T(128)} %param.10) | copy-start | bytes 1540
  6.5 26.0 %copy-start.2 = (f32[16]{0:T(128)S(1)}, f32[16]{0:T(128)}, u32[]{:S(2)}) copy-start(f32[16]{0:T(128)} %param.9) | copy-start | bytes 196
  6.5 160.3 %all-gather.2.cloned.1.call-start = ((), (), s32[]{:S(2)}) async-start(), calls=%async_computation.3 | async-start | bytes 17301504 | tf_op jit(solution)/shard_map/all_gather | solution.py:121
  9.9 16.3 %all-to-all-start = ((bf16[8,64,2,128]{3,1,2,0:T(8,128)(2,1)}), bf16[8,64,2,128]{3,1,2,0:T(8,128)(2,1)S(1)}, u32[]{:S(2)}, u32[]{:S(2)}) async-start(bf16[8,64,2,128]{3,1,2,0:T(8,128)(2,1)} %bitcast.1), calls=%async_computation | async-start | bytes 524288 | tf_op jit(solution)/shard_map/all_to_all | solution.py:46
  26.3 26.9 %all-to-all-start.1 = ((bf16[128,16,128]{0,2,1:T(8,128)(2,1)}), bf16[128,16,128]{0,2,1:T(8,128)(2,1)S(1)}, u32[]{:S(2)}, u32[]{:S(2)}) async-start(bf16[128,16,128]{0,2,1:T(8,128)(2,1)} %bitcast.10), calls=%async_computation.1 | async-start | bytes 1048576 | tf_op jit(solution)/shard_map/all_to_all | solution.py:98
  29.8 16.3 %collective-permute-start = (bf16[1,8,64,2,128]{4,2,3,1,0:T(8,128)(2,1)S(1)}, bf16[1,8,64,2,128]{4,2,3,1,0:T(8,128)(2,1)S(1)}, u32[]{:S(2)}, u32[]{:S(2)}) collective-permute-start(bf16[1,8,64,2,128]{4,2,3,1,0:T(8,128)(2,1)S(1)} %bitcast.118), channel_id=1, source_target_pairs={{0,4},{4,0},{8,12},{12,8},{16,20},{20,16},{24,28},{28,24},{1,5},{5... | collective-permute-start | bytes 786440 | tf_op jit(solution)/shard_map/ppermute | solution.py:22
  58.8 3.5 %copy-start.1 = (bf16[1024,2,32]{0,2,1:T(8,128)(2,1)S(1)}, bf16[1024,2,32]{0,2,1:T(8,128)(2,1)}, u32[]{:S(2)}) copy-start(bf16[1024,2,32]{0,2,1:T(8,128)(2,1)} %get-tuple-element.10) | copy-start | bytes 393220
Sparse Core Ops, SparseCore 0:
  10.2 156.6 all-gather.1
where the time goes:
time: 183 us
  waiting for transfers between devices  85.8 us (47%)
  blocking collectives  32.6 us (18%)
  matrix products  20.1 us (11%)
  between operations  13.6 us (7%)
  starting transfers between devices  12.8 us (7%)
  other arithmetic  11.4 us (6%)
  local copies, waits for them, and re-layouts  6.52 us (4%)
    all_gather x1, waiting for transfers between devices, shards(): lax.all_gather(out_weight, ('sp', 'dp'), axis=1, tiled=True)  59.7 us
    all_to_all x1, blocking collectives, shards(): lax.all_to_all(head_out.reshape(seqlen, per_device * VALUE_DIM), 'sp', sp...  32.6 us
    ppermute x1, waiting for transfers between devices, swapped(): return lax.ppermute(block, axis, route)  13.4 us
    sub x2, matrix products, attend(): raised = jnp.exp(scores - row_top)  9.88 us
    dot_general x1, matrix products, shards(): jnp.dot(heads_local, lax.all_gather(out_weight, ('sp', 'dp'), axis=1, til...  9.12 us
    div x2, other arithmetic, attend(): maps = raised / jnp.sum(raised, -1, keepdims=True)  7.49 us
    all_to_all x1, starting transfers between devices, gather_group(): lax.all_to_all(arranged, 'sp', split_axis=0, concat_axis=1, tiled=True)  7.31 us
    all_to_all x1, waiting for transfers between devices, gather_group(): lax.all_to_all(arranged, 'sp', split_axis=0, concat_axis=1, tiled=True)  6.03 us
  transfers between devices with their start and end apart: 4, of which 4 were waited for; matrix products, arithmetic and copies ran while one was open for 16% of the time, Pallas kernels for 0%

commit v1 on v0

--- a/solution.py
+++ b/solution.py
@@ -118,7 +118,7 @@
     )
     mixed = jnp.dot(
         heads_local,
-        lax.all_gather(out_weight, ("sp", "dp"), axis=1, tiled=True),
+        jnp.concatenate(lax.all_gather(out_weight, ("sp", "dp")), axis=1),
         preferred_element_type=jnp.float32,
     ).astype(jnp.bfloat16)
     return mixed[None]

time: 183 us -> 177 us (0.967)
  waiting for transfers between devices: 85.8 us -> 56.4 us
  local copies, waits for them, and re-layouts: 6.52 us -> 27.9 us
  matrix products: 20.1 us -> 23.4 us
  blocking collectives: 32.6 us -> 29.4 us
    all_gather x1, waiting for transfers between devices: 59.7 us -> 35.9 us  [shards(): lax.all_gather(out_weight, ('sp', 'dp'))]
    reshape x0 -> x1, local copies, waits for them, and re-layouts: none -> 21.4 us  [shards(): jnp.concatenate(lax.all_gather(out_weight, ('sp', 'dp')), axis=1)]
    ppermute x1, waiting for transfers between devices: 13.4 us -> 5.86 us  [swapped(): return lax.ppermute(block, axis, route)]
    dot_general x1, matrix products: 9.12 us -> 12.5 us  [shards(): jnp.dot(heads_local, jnp.concatenate(lax.all_gather(out_weight, ('sp', 'd...]
    all_to_all x1, blocking collectives: 32.6 us -> 29.4 us  [shards(): lax.all_to_all(head_out.reshape(seqlen, per_device * VALUE_DIM), 'sp', sp...]
where the time goes in v1:
time: 177 us; the launch traced here: 176 us
  waiting for transfers between devices  56.4 us (32%)
  blocking collectives  29.4 us (17%)
  local copies, waits for them, and re-layouts  27.9 us (16%)
  matrix products  23.4 us (13%)
  starting transfers between devices  13.9 us (8%)
  between operations  13.6 us (8%)
  other arithmetic  11.4 us (6%)
    all_gather x1, waiting for transfers between devices, shards(): lax.all_gather(out_weight, ('sp', 'dp'))  35.9 us
    all_to_all x1, blocking collectives, shards(): lax.all_to_all(head_out.reshape(seqlen, per_device * VALUE_DIM), 'sp', sp...  29.4 us
    reshape x1, local copies, waits for them, and re-layouts, shards(): jnp.concatenate(lax.all_gather(out_weight, ('sp', 'dp')), axis=1)  21.4 us
    dot_general x1, matrix products, shards(): jnp.dot(heads_local, jnp.concatenate(lax.all_gather(out_weight, ('sp', 'd...  12.5 us
    sub x2, matrix products, attend(): raised = jnp.exp(scores - row_top)  9.87 us
    div x2, other arithmetic, attend(): maps = raised / jnp.sum(raised, -1, keepdims=True)  7.5 us
    all_to_all x1, waiting for transfers between devices, gather_group(): lax.all_to_all(arranged, 'sp', split_axis=0, concat_axis=1, tiled=True)  7.43 us
    all_to_all x1, starting transfers between devices, gather_group(): lax.all_to_all(arranged, 'sp', split_axis=0, concat_axis=1, tiled=True)  7.31 us
  transfers between devices with their start and end apart: 4, of which 4 were waited for; matrix products, arithmetic and copies ran while one was open for 16% of the time, Pallas kernels for 0%

profile of v1, /device:TPU:0, one launch (start us, length us, event | category | flops | bytes accessed | tf_op | source)
XLA Modules:
  0.0 176.1 jit_solution(14576190459636888510)
XLA Ops:
  6.5 0.0 copy-start
  6.5 0.0 copy-start.3
  6.5 0.0 all-gather.3.cloned.1.call-start
  6.5 0.7 all-gather.3.cloned.1.call-update
  7.3 0.9 stack.7
  8.2 0.9 stack.8
  9.2 0.7 pad_maximum_fusion.3
  9.9 7.3 %all-to-all-start = ((bf16[8,64,2,128]{3,1,2,0:T(8,128)(2,1)}), bf16[8,64,2,128]{3,1,2,0:T(8,128)(2,1)S(1)}, u32[]{:S(2)}, u32[]{:S(2)}) async-start(bf16[8,64,2,128]{3,1,2,0:T(8,128)(2,1)} %bitcast.1), calls=%async_computation | async-start | bytes 524288 | tf_op jit(solution)/shard_map/all_to_all | solution.py:46
  17.2 2.0 %copy.41 = bf16[1,128,2048]{1,2,0:T(8,128)(2,1)} copy(bf16[1,128,2048]{2,1,0:T(8,128)(2,1)} %param.6) | data formatting | bytes 1048576 | tf_op args[0]
  19.3 0.5 fusion.39
  19.8 0.4 iota_compare_fusion
  20.2 7.4 %all-to-all-done = bf16[8,64,2,128]{3,1,2,0:T(8,128)(2,1)S(1)} async-done(((bf16[8,64,2,128]{3,1,2,0:T(8,128)(2,1)}), bf16[8,64,2,128]{3,1,2,0:T(8,128)(2,1)S(1)}, u32[]{:S(2)}, u32[]{:S(2)}) %all-to-all-start) | async-done | bytes 262176 | tf_op jit(solution)/shard_map/all_to_all | solution.py:46
  27.7 4.6 %all-to-all-start.1 = ((bf16[128,16,128]{0,2,1:T(8,128)(2,1)}), bf16[128,16,128]{0,2,1:T(8,128)(2,1)S(1)}, u32[]{:S(2)}, u32[]{:S(2)}) async-start(bf16[128,16,128]{0,2,1:T(8,128)(2,1)} %bitcast.10), calls=%async_computation.1 | async-start | bytes 1048576 | tf_op jit(solution)/shard_map/all_to_all | solution.py:98
  32.2 2.0 %collective-permute-start = (bf16[1,8,64,2,128]{4,2,3,1,0:T(8,128)(2,1)S(1)}, bf16[1,8,64,2,128]{4,2,3,1,0:T(8,128)(2,1)S(1)}, u32[]{:S(2)}, u32[]{:S(2)}) collective-permute-start(bf16[1,8,64,2,128]{4,2,3,1,0:T(8,128)(2,1)S(1)} %bitcast.124), channel_id=1, source_target_pairs={{0,4},{4,0},{8,12},{12,8},{16,20},{20,16},{24,28},{28,24},{1,5},{5... | collective-permute-start | bytes 786440 | tf_op jit(solution)/shard_map/ppermute | solution.py:22
  34.3 0.0 copy-done
  34.3 0.8 iota_compare_fusion.1
  35.0 0.0 copy-done.3
  35.0 0.1 dynamic_slice.3
  35.1 5.9 %collective-permute-done = bf16[1,8,64,2,128]{4,2,3,1,0:T(8,128)(2,1)S(1)} collective-permute-done((bf16[1,8,64,2,128]{4,2,3,1,0:T(8,128)(2,1)S(1)}, bf16[1,8,64,2,128]{4,2,3,1,0:T(8,128)(2,1)S(1)}, u32[]{:S(2)}, u32[]{:S(2)}) %collective-permute-start) | collective-permute-done | bytes 262176 | tf_op jit(solution)/shard_map/ppermute | solution.py:22
  41.0 0.1 maximum_bitcast_fusion
  41.2 0.2 copy.40
  41.4 0.7 subtract_convert_fusion.1
  42.1 6.5 %all-to-all-done.1 = bf16[128,16,128]{0,2,1:T(8,128)(2,1)S(1)} async-done(((bf16[128,16,128]{0,2,1:T(8,128)(2,1)}), bf16[128,16,128]{0,2,1:T(8,128)(2,1)S(1)}, u32[]{:S(2)}, u32[]{:S(2)}) %all-to-all-start.1) | async-done | bytes 524320 | tf_op jit(solution)/shard_map/all_to_all | solution.py:98
  48.6 0.1 convert_element_type.55
  48.7 0.6 copy.43
  49.3 0.2 reshape.184
  49.5 0.1 fusion.63
  49.6 0.1 subtract_convert_fusion
  49.7 4.5 %fusion.69 = (f32[2,2,512]{2,0,1:T(2,128)S(1)}, f32[2,2,512,512]{2,3,0,1:T(8,128)}) fusion(pred[512,512]{0,1:T(8,128)(4,1)} %iota_compare_fusion.1, bf16[1024,2,32]{0,2,1:T(8,128)(2,1)S(1)} %get-tuple-element.9, bf16[1024,2,32]{0,2,1:T(8,128)(2,1)} %get-tuple-element.10, bf16[1024,2,2,32]{0,3,1,2:T(8,128)(2,1)S(1)} %get-tuple-element.5, ...), kind=kOutput, calls=%fused_computation.77 | convolution fusion | flops 139198976 | bytes 5251072 | tf_op jit(solution)/shard_map/sub | solution.py:78
  54.3 0.0 copy-start.2
  54.3 3.0 %broadcast_divide_fusion.1 = f32[2,2,512,512]{2,3,0,1:T(8,128)S(1)} fusion(f32[2,2,512,512]{2,3,0,1:T(8,128)} %get-tuple-element.18, f32[2,2,512]{2,0,1:T(2,128)S(1)} %get-tuple-element.17), kind=kLoop, calls=%fused_computation.22 | loop fusion | flops 1048576 | bytes 8396800 | tf_op jit(solution)/shard_map/div | solution.py:79
  57.3 0.4 fusion.19
  57.7 0.0 copy-done.2
  57.8 5.3 %fusion.64 = (f32[2,2,512]{2,0,1:T(2,128)S(1)}, f32[2,2,512,1024]{2,3,0,1:T(8,128)}) fusion(pred[512,1024]{0,1:T(8,128)(4,1)S(1)} %iota_compare_fusion, bf16[1024,2,32]{0,2,1:T(8,128)(2,1)S(1)} %copy-done.2, bf16[1024,2,32]{0,2,1:T(8,128)(2,1)S(1)} %get-tuple-element.9, bf16[1024,2,2,32]{0,3,1,2:T(8,128)(2,1)S(1)} %get-tuple-element.6, ...), kind=kOutput, calls=%fused_computation.76 | convolution fusion | flops 277873664 | bytes 9707520 | tf_op jit(solution)/shard_map/sub | solution.py:78
  63.1 4.5 %broadcast_divide_fusion = f32[2,2,512,1024]{2,3,0,1:T(8,128)S(1)} fusion(f32[2,2,512,1024]{2,3,0,1:T(8,128)} %get-tuple-element.16, f32[2,2,512]{2,0,1:T(2,128)S(1)} %get-tuple-element.15), kind=kLoop, calls=%fused_computation.11 | loop fusion | flops 2097152 | bytes 16785408 | tf_op jit(solution)/shard_map/div | solution.py:79
  67.6 0.6 fusion.15
  68.2 0.1 fusion.21
  68.3 0.1 mul.266
  68.4 0.2 copy.63
  68.6 0.4 copy.51
  69.0 0.2 copy.49
  69.2 0.2 copy.50
  69.4 0.1 pad_maximum_fusion
  69.5 0.2 multiply_convert_fusion
  69.7 29.4 %all_to_all.34 = bf16[8,128,256]{2,1,0:T(8,128)(2,1)S(1)} all-to-all(bf16[8,128,256]{2,1,0:T(8,128)(2,1)S(1)} %multiply_convert_fusion), channel_id=1, replica_groups=mesh['sp'=8,'dp'=4] {'sp'}, dimensions={0} | all-to-all | bytes 1048576 | tf_op jit(solution)/shard_map/all_to_all | solution.py:112
  99.1 0.3 copy.52
  99.4 35.9 %all-gather.3.cloned.1.call-done = bf16[65536,128]{1,0:T(8,128)(2,1)} async-done(((bf16[2048,128]{1,0:T(8,128)(2,1)}), bf16[65536,128]{1,0:T(8,128)(2,1)}) %all-gather.3.cloned.1.call-update) | async-done | bytes 16777232 | tf_op jit(solution)/shard_map/all_gather | solution.py:121
  135.3 21.4 %copy.53 = bf16[2048,32,128]{0,2,1:T(8,128)(2,1)} copy(bf16[2048,32,128]{2,0,1:T(8,128)(2,1)} %bitcast.109) | data formatting | bytes 33554432 | tf_op jit(solution)/shard_map/reshape | solution.py:121
  156.7 0.0 copy-start.1
  156.7 12.5 %fusion.3 = bf16[1,128,4096]{2,1,0:T(8,128)(2,1)} fusion(bf16[128,2048]{0,1:T(8,128)(2,1)S(1)} %bitcast.121, bf16[2048,4096]{0,1:T(8,128)(2,1)} %bitcast.108), kind=kOutput, calls=%fused_computation.6 | convolution fusion | flops 2148007936 | bytes 18350080 | tf_op jit(solution)/shard_map/dot_general | solution.py:119
  169.2 0.0 copy-done.1
  (9 shorter events, 0.2 us)
Async XLA Ops:
  6.5 27.7 %copy-start = (f32[128]{0:T(128)S(1)}, f32[128]{0:T(128)}, u32[]{:S(2)}) copy-start(f32[128]{0:T(128)} %param.10) | copy-start | bytes 1540
  6.5 28.5 %copy-start.3 = (f32[16]{0:T(128)S(1)}, f32[16]{0:T(128)}, u32[]{:S(2)}) copy-start(f32[16]{0:T(128)} %param.9) | copy-start | bytes 196
  6.5 128.8 %all-gather.3.cloned.1.call-start = ((), (), s32[]{:S(2)}) async-start(), calls=%async_computation.3 | async-start | bytes 17301504 | tf_op jit(solution)/shard_map/all_gather | solution.py:121
  9.9 17.7 %all-to-all-start = ((bf16[8,64,2,128]{3,1,2,0:T(8,128)(2,1)}), bf16[8,64,2,128]{3,1,2,0:T(8,128)(2,1)S(1)}, u32[]{:S(2)}, u32[]{:S(2)}) async-start(bf16[8,64,2,128]{3,1,2,0:T(8,128)(2,1)} %bitcast.1), calls=%async_computation | async-start | bytes 524288 | tf_op jit(solution)/shard_map/all_to_all | solution.py:46
  27.7 20.9 %all-to-all-start.1 = ((bf16[128,16,128]{0,2,1:T(8,128)(2,1)}), bf16[128,16,128]{0,2,1:T(8,128)(2,1)S(1)}, u32[]{:S(2)}, u32[]{:S(2)}) async-start(bf16[128,16,128]{0,2,1:T(8,128)(2,1)} %bitcast.10), calls=%async_computation.1 | async-start | bytes 1048576 | tf_op jit(solution)/shard_map/all_to_all | solution.py:98
  32.2 8.7 %collective-permute-start = (bf16[1,8,64,2,128]{4,2,3,1,0:T(8,128)(2,1)S(1)}, bf16[1,8,64,2,128]{4,2,3,1,0:T(8,128)(2,1)S(1)}, u32[]{:S(2)}, u32[]{:S(2)}) collective-permute-start(bf16[1,8,64,2,128]{4,2,3,1,0:T(8,128)(2,1)S(1)} %bitcast.124), channel_id=1, source_target_pairs={{0,4},{4,0},{8,12},{12,8},{16,20},{20,16},{24,28},{28,24},{1,5},{5... | collective-permute-start | bytes 786440 | tf_op jit(solution)/shard_map/ppermute | solution.py:22
  54.3 3.5 %copy-start.2 = (bf16[1024,2,32]{0,2,1:T(8,128)(2,1)S(1)}, bf16[1024,2,32]{0,2,1:T(8,128)(2,1)}, u32[]{:S(2)}) copy-start(bf16[1024,2,32]{0,2,1:T(8,128)(2,1)} %get-tuple-element.10) | copy-start | bytes 393220
  156.7 12.5 %copy-start.1 = (f32[128]{0:T(128)S(1)}, f32[128]{0:T(128)}, u32[]{:S(2)}) copy-start(f32[128]{0:T(128)} %param.10) | copy-start | bytes 1540
Sparse Core Ops, SparseCore 0:
  10.2 125.0 all-gather.2
